TPU v7x, 32 devices: a whole 2x2x4 slice. The times are simulated.
32 devices in a mesh: ep: 4 (over y, x), tp: 8 (over z, core).
Axes of the slice: x: 2, y: 2, z: 4, core: 2. Of those that a mesh axis runs over, the one named last changes fastest.
Arguments:
- queries: bfloat16 [16, 64, 2, 512], P('tp', None, None, 'ep'), may hold values from -24 to 24
- key_vectors: bfloat16 [16, 64, 2, 512], P('tp', None, None, 'ep'), may hold values from -24 to 24
- value_vectors: bfloat16 [16, 64, 2, 512], P('tp', None, None, 'ep'), may hold values from -6 to 6
- mixer_weight: bfloat16 [1024, 2048], replicated, may hold values from -0.375 to 0.375
- expert_rows: bfloat16 [512, 2048], P('ep'), may hold values from -6 to 6
- norm_gain: float32 [2048], replicated, may hold values from 0.1 to 1.9
- route_ids: int32 [512, 2], P('ep'), may hold values from 0 to 7, all different within a row; in each aligned block of 128 rows (0 to 127, 128 to 255, ...) at most 64 rows name the same one
- route_logits: float32 [512, 2], P('ep'), may hold values from -4 to 4
- gate_weight: bfloat16 [8, 2048, 4096], P('ep', None, 'tp'), may hold values from -0.39648438 to 0.39648438
- up_weight: bfloat16 [8, 2048, 4096], P('ep', None, 'tp'), may hold values from -0.39648438 to 0.39648438
- down_weight: bfloat16 [8, 4096, 2048], P('ep', 'tp'), may hold values from -0.028076172 to 0.028076172
Outputs:
- mixer_out: bfloat16 [2, 512, 2048], P(None, ('ep', 'tp'))
- routed_out: bfloat16 [2048, 512], P('tp', 'ep')
Inputs may be any that keep to these rules, and one draw needn't show every extreme that they name: `route_ids`: each row names 2 different experts. Among the 128 rows of one index of ep no expert is named more than 64 times, a bound that some expert reaches in such a block.
All inputs are finite; a program needn't handle non-finite values.
Results may differ from a plain program's by a relative error of at most 0.018.
Values may be sent and summed in bfloat16 or wider, within the bound.
A program may use at most 64 MiB of HBM per device.

v0:
```python
import jax
import jax.numpy as jnp
from jax import lax
from jax.sharding import PartitionSpec as P

limit_value = 7.0
alpha_value = 1.702
norm_eps = 1e-06


def activate(gate_pre, up_pre):
    gate_clamped = jnp.minimum(gate_pre, limit_value)
    up_clamped = jnp.clip(up_pre, -limit_value, limit_value)
    return ((up_clamped + 1.0) * gate_clamped * jax.nn.sigmoid(alpha_value * gate_clamped)).astype(
        jnp.bfloat16
    )


def block_terms(query_rows, key_block, value_block, block_index, own_index):
    seg_len = query_rows.shape[3]
    score_scale = query_rows.shape[1] ** (-0.5)
    scores = (
        jnp.einsum("hdsq,hdsk->hsqk", query_rows, key_block, preferred_element_type=jnp.float32)
        * score_scale
    )
    query_pos = lax.broadcasted_iota(jnp.int32, (seg_len, seg_len), 0)
    lookup_slot = lax.broadcasted_iota(jnp.int32, (seg_len, seg_len), 1)
    usable = jnp.logical_or(block_index < own_index, lookup_slot < query_pos)
    log_keep = jnp.where(usable, jax.nn.log_sigmoid(-scores), 0.0)
    within = lax.cumsum(log_keep, axis=3, reverse=True) - log_keep
    weight = jnp.where(usable, jnp.exp(jax.nn.log_sigmoid(scores) + within), 0.0).astype(
        jnp.bfloat16
    )
    block_out = jnp.einsum(
        "hsqk,hdsk->hdsq", weight, value_block, preferred_element_type=jnp.float32
    )
    return (block_out, jnp.sum(log_keep, axis=3))


def attend(query_rows, key_vectors, value_vectors):
    head_count, head_dim, seq_count, seg_len = query_rows.shape
    blocks = lax.axis_size("ep")
    own_index = lax.axis_index("ep")
    first_outs = jnp.zeros((blocks, head_count, head_dim, seq_count, seg_len), jnp.float32)
    first_totals = jnp.zeros((blocks, head_count, seq_count, seg_len), jnp.float32)
    key_piece = lax.all_gather(key_vectors, "ep", axis=3, tiled=True)
    value_piece = lax.all_gather(value_vectors, "ep", axis=3, tiled=True)
    shard_count = key_piece.shape[3] // seg_len

    def one_block(offset, inner_state):
        block_outs, block_totals = inner_state
        key_block = lax.dynamic_slice_in_dim(key_piece, offset * seg_len, seg_len, 3)
        value_block = lax.dynamic_slice_in_dim(value_piece, offset * seg_len, seg_len, 3)

        def compute(unused):
            return block_terms(query_rows, key_block, value_block, offset, own_index)

        def skip_block(unused):
            return (
                jnp.zeros((head_count, head_dim, seq_count, seg_len), jnp.float32),
                jnp.zeros((head_count, seq_count, seg_len), jnp.float32),
            )

        block_out, block_total = lax.cond(offset <= own_index, compute, skip_block, 0)
        block_outs = lax.dynamic_update_index_in_dim(block_outs, block_out, offset, 0)
        block_totals = lax.dynamic_update_index_in_dim(block_totals, block_total, offset, 0)
        return (block_outs, block_totals)

    block_outs, block_totals = lax.fori_loop(0, shard_count, one_block, (first_outs, first_totals))
    later_sums = lax.cumsum(block_totals, axis=0, reverse=True) - block_totals
    return jnp.sum(jnp.exp(later_sums)[:, :, None] * block_outs, axis=0).astype(jnp.bfloat16)


def mix_heads(attended, mixer_weight):
    head_count, head_dim, seq_count, seg_len = attended.shape
    flat_heads = attended.reshape(head_count * head_dim, seq_count, seg_len)
    return jnp.einsum(
        "csr,cm->srm",
        lax.all_to_all(flat_heads, "tp", split_axis=2, concat_axis=0, tiled=True),
        mixer_weight,
        preferred_element_type=jnp.float32,
    ).astype(jnp.bfloat16)


def expert_block(send_rows, gate_portion, up_part, down_part):
    groups = lax.axis_size("ep")
    local_experts = gate_portion.shape[0]
    cap_rows = send_rows.shape[1]
    model_width = send_rows.shape[2]
    received = lax.all_to_all(send_rows, "ep", split_axis=0, concat_axis=0, tiled=True)
    bucketed = received.reshape(groups, local_experts, cap_rows, model_width)
    gate_pre = jnp.einsum(
        "sjcd,jdf->sjcf", bucketed, gate_portion, preferred_element_type=jnp.float32
    )
    up_pre = jnp.einsum("sjcd,jdf->sjcf", bucketed, up_part, preferred_element_type=jnp.float32)
    hidden = activate(gate_pre, up_pre)
    slot_total = groups * local_experts * cap_rows
    term_rows = jnp.einsum("sjcf,jfd->dsjc", hidden, down_part, preferred_element_type=jnp.float32)
    summed = lax.psum_scatter(
        term_rows.reshape(
            model_width // lax.axis_size("tp") * lax.axis_size("tp"), slot_total
        ).astype(jnp.bfloat16),
        "tp",
        scatter_dimension=0,
        tiled=True,
    ).astype(jnp.float32)
    return lax.all_to_all(
        summed.astype(jnp.bfloat16), "ep", split_axis=1, concat_axis=1, tiled=True
    ).astype(summed.dtype)


def route_experts(
    expert_rows, norm_gain, route_ids, route_logits, gate_weight, up_weight, down_weight
):
    groups = lax.axis_size("ep")
    local_experts = gate_weight.shape[0]
    expert_count = groups * local_experts
    token_rows, top_count = route_ids.shape
    cap_rows = 2 * token_rows * top_count // expert_count
    values = expert_rows.astype(jnp.float32)
    scaled = values * lax.rsqrt(jnp.mean(values * values, axis=-1, keepdims=True) + norm_eps)
    normed = (scaled * norm_gain).astype(jnp.bfloat16)
    route_weight = jax.nn.softmax(route_logits, axis=-1)
    flat_ids = route_ids.reshape(token_rows * top_count)
    one_hot_matrix = (
        flat_ids[:, None] == jnp.arange(expert_count, dtype=jnp.int32)[None, :]
    ).astype(jnp.int32)
    earlier = jnp.cumsum(one_hot_matrix, axis=0) - one_hot_matrix
    slot_rank = jnp.sum(earlier * one_hot_matrix, axis=1)
    column = flat_ids * cap_rows + slot_rank
    token_index = jnp.arange(token_rows * top_count, dtype=jnp.int32) // top_count
    owner_token = jnp.zeros((expert_count * cap_rows,), jnp.int32).at[column].set(token_index)
    filled = jnp.zeros((expert_count * cap_rows,), jnp.int32).at[column].set(1)
    send_rows = jnp.where(filled[:, None] > 0, normed[owner_token], jnp.zeros((), jnp.bfloat16))
    send_rows = send_rows.reshape(groups, local_experts, cap_rows, normed.shape[1])
    halves = 1
    per_half = local_experts // halves
    part_rows = send_rows.reshape(groups * per_half, cap_rows, normed.shape[1])
    result = expert_block(part_rows, gate_weight, up_weight, down_weight)
    results = result.reshape(result.shape[0], groups, per_half, cap_rows)
    gathered = results.reshape(results.shape[0], expert_count * cap_rows)
    picked = jnp.take(gathered, column, axis=1).reshape(gathered.shape[0], token_rows, top_count)
    combined = jnp.sum(picked * route_weight[None], axis=2)
    return combined.astype(jnp.bfloat16)


def body(
    queries,
    key_vectors,
    value_vectors,
    mixer_weight,
    expert_rows,
    norm_gain,
    route_ids,
    route_logits,
    gate_weight,
    up_weight,
    down_weight,
):
    attended = attend(queries, key_vectors, value_vectors)
    mixer_out = mix_heads(attended, mixer_weight)
    routed_out = route_experts(
        expert_rows, norm_gain, route_ids, route_logits, gate_weight, up_weight, down_weight
    )
    return (mixer_out, routed_out)


def solution(mesh):
    in_specs = (
        P("tp", None, None, "ep"),
        P("tp", None, None, "ep"),
        P("tp", None, None, "ep"),
        P(),
        P("ep", None),
        P(),
        P("ep", None),
        P("ep", None),
        P("ep", None, "tp"),
        P("ep", None, "tp"),
        P("ep", "tp", None),
    )
    out_specs = (P(None, ("ep", "tp"), None), P("tp", "ep"))
    return jax.shard_map(body, mesh=mesh, in_specs=in_specs, out_specs=out_specs, check_vma=False)
```

profile of v0, /device:TPU:0, one launch (start us, length us, event | category | flops | bytes accessed | tf_op | source)
XLA Modules:
  0.0 130.4 jit_solution(11275441368211532716)
XLA Ops:
  7.2 0.0 reduce-scatter.2.cloned.1.call-start
  7.2 0.8 copy.67
  8.0 0.1 eq.26
  8.1 0.1 reshape.99
  8.3 0.7 broadcast_multiply_fusion
  9.0 0.6 reduce-window.6
  9.6 0.2 slice_reduce_fusion
  9.8 0.1 copy.71
  9.9 0.1 mul.98
  10.1 0.1 fusion.87
  10.2 1.4 %scatter_custom_fusion.1 = s32[512]{0:T(512)S(1)} fusion(s32[256]{0:T(256)S(1)} %bitcast.93, s32[256]{0:T(256)S(1)} %and_select_fusion, s32[]{:T(128)} %copy.121), kind=kCustom, calls=%fused_computation.82 | custom fusion | bytes 2052 | tf_op jit(solution)/shard_map/scatter | solution.py:132
  11.6 1.2 fusion.73
  12.8 1.4 %scatter_custom_fusion = s32[512]{0:T(512)S(1)} fusion(s32[256]{0:T(256)S(1)} %bitcast.94, s32[256]{0:T(256)S(1)} %broadcast.130, s32[]{:T(128)} %copy.121), kind=kCustom, calls=%fused_computation.85 | custom fusion | bytes 2052 | tf_op jit(solution)/shard_map/scatter | solution.py:133
  14.3 0.1 broadcast_in_dim.94
  14.3 1.2 fusion.75
  15.6 2.5 %gather_fusion = bf16[512,2048]{1,0:T(8,128)(2,1)S(1)} fusion(bf16[128,2048]{1,0:T(8,128)(2,1)S(1)} %fusion.75, s32[1024]{0:T(1024)S(1)} %pad_clamp_fusion.1), kind=kCustom, calls=%fused_computation | custom fusion | bytes 4196352 | tf_op jit(solution)/shard_map/gather | solution.py:134
  18.1 0.2 broadcast_select_fusion
  18.3 30.6 %all_to_all.32 = bf16[8,64,2048]{2,1,0:T(8,128)(2,1)S(1)} all-to-all(bf16[8,64,2048]{2,1,0:T(8,128)(2,1)S(1)} %broadcast_select_fusion), channel_id=1, replica_groups=mesh['ep'=4,'tp'=8] {'ep'}, dimensions={0} | all-to-all | bytes 4194304 | tf_op jit(solution)/shard_map/all_to_all | solution.py:90
  48.9 1.2 fusion.57
  50.2 7.3 %fusion.29 = bf16[2048,4,2,64]{0,3,1,2:T(8,128)(2,1)} fusion(bf16[2,512,2048]{2,1,0:T(8,128)(2,1)} %param.25, f32[2,4,64,512]{3,2,1,0:T(8,128)S(1)} %fusion.57, bf16[2,2048,512]{2,1,0:T(8,128)(2,1)} %param.24, bf16[4,2,64,2048]{3,2,1,0:T(8,128)(2,1)S(1)} %bitcast.86), kind=kOutput, calls=%fused_computation.36 | convolution fusion | flops 2150891520 | bytes 13631488 | tf_op jit(solution)/shard_map/sjcf,jfd->dsjc/dot_general | solution.py:98
  57.4 3.2 %copy.74 = bf16[2048,4,2,64]{0,3,2,1:T(8,128)(2,1)} copy(bf16[2048,4,2,64]{0,3,1,2:T(8,128)(2,1)} %fusion.29) | data formatting | bytes 4194304 | tf_op jit(solution)/shard_map/convert_element_type | solution.py:102
  60.6 0.0 reduce-scatter.2.cloned.1.call-update
  60.7 0.8 copy-done
  61.5 0.0 copy-done.1
  61.5 0.0 copy-done.2
  61.6 8.6 %all_gather.6 = bf16[2,64,2,512]{3,1,2,0:T(8,128)(2,1)S(1)} all-gather(bf16[2,64,2,128]{3,1,2,0:T(8,128)(2,1)S(1)} %copy.60), channel_id=1, replica_groups=mesh['ep'=4,'tp'=8] {'ep'}, dimensions={3}, use_global_device_ids=true | all-gather | bytes 327680 | tf_op jit(solution)/shard_map/all_gather | solution.py:46
  70.2 8.9 %all_gather.7 = bf16[2,64,2,512]{3,1,2,0:T(8,128)(2,1)S(1)} all-gather(bf16[2,64,2,128]{3,1,2,0:T(8,128)(2,1)S(1)} %copy.61), channel_id=1, replica_groups=mesh['ep'=4,'tp'=8] {'ep'}, dimensions={3}, use_global_device_ids=true | all-gather | bytes 327680 | tf_op jit(solution)/shard_map/all_gather | solution.py:47
  79.1 5.8 %while.15 = (s32[]{:T(128)}, f32[4,2,64,2,128]{4,2,3,1,0:T(8,128)S(1)}, f32[4,2,2,128]{3,2,1,0:T(2,128)S(1)}, s32[]{:T(128)}, bf16[2,64,2,512]{3,1,2,0:T(8,128)(...) while((s32[]{:T(128)}, ...), condition=%wide.region_5.6_spmd, body=%wide.region_0.5_spmd.sunk | while | flops 27098632 | bytes 2218215 | solution.py:69
  79.1 5.4 %conditional.2 = (f32[1,2,64,2,128]{4,2,3,1,0:T(8,128)S(1)}, f32[1,2,2,128]{3,2,1,0:T(2,128)S(1)}) conditional(s32[]{:T(128)} %convert_element_type.99, () %tuple.66, (s32[]{:T(128)}, s32[]{:T(128)}, bf16[2,64,2,512]{3,1,2,0:T(8,128)(2,1)S(1)}, bf16[2,64,2,128]{3,1,2,0:T(8,128)(2,1)S(1)}, bf16[2,64,2,512]{3,1,2,0:T(8,128)(2,1)S(1)}) %tuple.67), branch_computations={%region_1.0_spmd, %region_2.4_spmd} | conditional | flops 27098628 | bytes 1951828 | solution.py:64
  79.1 0.4 fusion.16
  79.5 4.4 %reduce_window_sum.35 = f32[2,2,128,128]{2,3,1,0:T(8,128)S(1)} reduce-window(f32[2,2,128,128]{2,3,1,0:T(8,128)S(1)} %get-tuple-element.277, f32[]{:T(128)} %constant.130.clone), window={size=1x1x1x128 pad=0_0x0_0x0_0x0_127}, to_apply=%region_3.2 | reduce-window | flops 8323072 | bytes 524292 | tf_op jit(solution)/shard_map/while/body/eval_jaxpr/cond/branch_1_fun/reduce_window_sum | solution.py:30
  84.0 0.5 convolution_bitcast_fusion
  84.9 0.8 copy.64
  85.7 4.9 %all-to-all-start = ((bf16[128,2,128]{0,1,2:T(2,128)(2,1)}), bf16[128,2,128]{0,1,2:T(2,128)(2,1)S(1)}, u32[]{:S(2)}, u32[]{:S(2)}) async-start(bf16[128,2,128]{0,1,2:T(2,128)(2,1)} %copy.64), calls=%async_computation | async-start | bytes 131072 | tf_op jit(solution)/shard_map/all_to_all | solution.py:79
  90.6 0.1 reduce_sum.64
  90.7 0.1 copy.69
  90.9 0.1 copy.70
  91.0 0.1 copy.75
  91.1 5.4 %all-to-all-done = bf16[128,2,128]{0,1,2:T(2,128)(2,1)S(1)} async-done(((bf16[128,2,128]{0,1,2:T(2,128)(2,1)}), bf16[128,2,128]{0,1,2:T(2,128)(2,1)S(1)}, u32[]{:S(2)}, u32[]{:S(2)}) %all-to-all-start) | async-done | bytes 65568 | tf_op jit(solution)/shard_map/all_to_all | solution.py:79
  96.5 0.3 reduce-scatter.2.cloned.1.call-done
  96.8 18.6 %all-to-all-start.2 = ((bf16[256,4,128]{0,2,1:T(8,128)(2,1)}), bf16[256,4,128]{0,2,1:T(8,128)(2,1)S(1)}, u32[]{:S(2)}, u32[]{:S(2)}) async-start(bf16[256,4,128]{0,2,1:T(8,128)(2,1)} %bitcast.89), calls=%async_computation.3 | async-start | bytes 524288 | tf_op jit(solution)/shard_map/all_to_all | solution.py:107
  115.3 3.7 %fusion.32 = bf16[2,16,2048]{2,1,0:T(8,128)(2,1)} fusion(bf16[1024,2048]{1,0:T(8,128)(2,1)} %param.18, bf16[2,8,2,8,128]{4,3,2,1,0:T(8,128)(2,1)S(1)} %bitcast.88), kind=kOutput, calls=%fused_computation.37 | convolution fusion | flops 134283264 | bytes 4390912 | tf_op jit(solution)/shard_map/csr,cm->srm/dot_general | solution.py:77
  119.0 1.7 %all-to-all-done.2 = bf16[256,4,128]{0,2,1:T(8,128)(2,1)S(1)} async-done(((bf16[256,4,128]{0,2,1:T(8,128)(2,1)}), bf16[256,4,128]{0,2,1:T(8,128)(2,1)S(1)}, u32[]{:S(2)}, u32[]{:S(2)}) %all-to-all-start.2) | async-done | bytes 262176 | tf_op jit(solution)/shard_map/all_to_all | solution.py:107
  120.7 0.1 bitcast_convert_fusion
  120.8 1.0 gather_fusion.1
  121.7 0.1 gather.14
  121.9 0.9 multiply_reduce_fusion.1
  122.8 0.7 copy.76
  (51 shorter events, 0.6 us)
Async XLA Ops:
  7.2 89.6 %reduce-scatter.2.cloned.1.call-start = ((), (), s32[]{:S(2)}) async-start(), calls=%async_computation.4 | async-start | bytes 2359296 | tf_op jit(solution)/shard_map/reduce_scatter | solution.py:99
  18.3 30.6 %copy-start.5 = (bf16[2,2048,512]{2,1,0:T(8,128)(2,1)S(1)}, bf16[2,2048,512]{2,1,0:T(8,128)(2,1)}, u32[]{:S(2)}) copy-start(bf16[2,2048,512]{2,1,0:T(8,128)(2,1)} %param.23) | copy-start | bytes 12582916
  60.6 0.8 copy-start
  60.6 0.9 copy-start.1
  60.6 0.9 copy-start.2
  79.0 11.7 %copy-start.4 = (f32[128,2]{0,1:T(2,128)S(1)}, f32[128,2]{0,1:T(2,128)}, u32[]{:S(2)}) copy-start(f32[128,2]{0,1:T(2,128)} %param.22) | copy-start | bytes 3076
  79.1 11.8 %copy-start.3 = (s32[128,2]{0,1:T(2,128)S(1)}, s32[128,2]{0,1:T(2,128)}, u32[]{:S(2)}) copy-start(s32[128,2]{0,1:T(2,128)} %param.21) | copy-start | bytes 3076
  85.7 10.8 %all-to-all-start = ((bf16[128,2,128]{0,1,2:T(2,128)(2,1)}), bf16[128,2,128]{0,1,2:T(2,128)(2,1)S(1)}, u32[]{:S(2)}, u32[]{:S(2)}) async-start(bf16[128,2,128]{0,1,2:T(2,128)(2,1)} %copy.64), calls=%async_computation | async-start | bytes 131072 | tf_op jit(solution)/shard_map/all_to_all | solution.py:79
  96.8 23.9 %all-to-all-start.2 = ((bf16[256,4,128]{0,2,1:T(8,128)(2,1)}), bf16[256,4,128]{0,2,1:T(8,128)(2,1)S(1)}, u32[]{:S(2)}, u32[]{:S(2)}) async-start(bf16[256,4,128]{0,2,1:T(8,128)(2,1)} %bitcast.89), calls=%async_computation.3 | async-start | bytes 524288 | tf_op jit(solution)/shard_map/all_to_all | solution.py:107
Sparse Core Ops, SparseCore 0:
  60.8 35.9 reduce-scatter.1
where the time goes:
time: 131 us; the launch traced here: 130 us
  blocking collectives  48.1 us (37%)
  starting transfers between devices  23.5 us (18%)
  between operations  14.3 us (11%)
  local copies, waits for them, and re-layouts  14.2 us (11%)
  matrix products  13.1 us (10%)
  other arithmetic  9.63 us (7%)
  waiting for transfers between devices  7.31 us (6%)
    all_to_all x1, blocking collectives, expert_block(): lax.all_to_all(send_rows, 'ep', split_axis=0, concat_axis=0, tiled=True)  30.6 us
    all_to_all x1, starting transfers between devices, expert_block(): lax.all_to_all(summed.astype(jnp.bfloat16), 'ep', split_axis=1, concat_ax...  18.6 us
    all_gather x1, blocking collectives, attend(): value_piece = lax.all_gather(value_vectors, 'ep', axis=3, tiled=True)  8.89 us
    all_gather x1, blocking collectives, attend(): key_piece = lax.all_gather(key_vectors, 'ep', axis=3, tiled=True)  8.6 us
    dot_general x1, matrix products, expert_block(): jnp.einsum('sjcf,jfd->dsjc', hidden, down_part, preferred_element_type=jn...  7.28 us
    all_to_all x1, waiting for transfers between devices, mix_heads(): lax.all_to_all(flat_heads, 'tp', split_axis=2, concat_axis=0, tiled=True)  5.35 us
    all_to_all x1, starting transfers between devices, mix_heads(): lax.all_to_all(flat_heads, 'tp', split_axis=2, concat_axis=0, tiled=True)  4.88 us
    another operation x1, other arithmetic, block_terms(): within = lax.cumsum(log_keep, axis=3, reverse=True) - log_keep  4.43 us
  transfers between devices with their start and end apart: 3, of which 3 were waited for; matrix products, arithmetic and copies ran while one was open for 8% of the time, Pallas kernels for 0%

commit v1 on v0

v1 whole, which is shorter than its diff:
```python
import functools

import jax
import jax.numpy as jnp
from jax import lax
from jax.experimental import pallas as pl
from jax.experimental.pallas import tpu as pltpu
from jax.sharding import PartitionSpec as P

limit_value = 7.0
alpha_value = 1.702
norm_eps = 1e-06

MESH = pl.DeviceIdType.MESH
f32 = jnp.float32
bf16 = jnp.bfloat16


def activate(gate_pre, up_pre):
    g = jnp.minimum(gate_pre, limit_value)
    u = jnp.clip(up_pre, -limit_value, limit_value)
    return ((u + 1.0) * g / (1.0 + jnp.exp(-alpha_value * g))).astype(bf16)


def partner_of(me, offset, count):
    other = me
    bit = 1
    while bit < count:
        set_bit = (offset // bit) % 2
        other = other + set_bit * bit * (1 - 2 * ((me // bit) % 2))
        bit *= 2
    return other


def kernel(
    n_ep,
    n_tp,
    qt_ref,
    kv_ref,
    x_ref,
    gain_ref,
    wt_ref,
    gate_hbm,
    up_hbm,
    down_hbm,
    mixer_hbm,
    mix_out,
    routed_out,
    wg,
    wu,
    wd,
    wm,
    xr,
    wr,
    xn,
    kvr,
    pb,
    cr,
    sb,
    rr,
    zb,
    zr,
    at_send,
    at_recv,
    w_sem,
    x_ss,
    x_rs,
    wt_ss,
    wt_rs,
    f_ss,
    f_rs,
    kv_ss,
    kv_rs,
    c_ss,
    c_rs,
    r_ss,
    r_rs,
    z_ss,
    z_rs,
    a_ss,
    a_rs,
):
    e = lax.axis_index("ep")
    t = lax.axis_index("tp")
    core = t % 2
    zi = t // 2
    zs = n_tp // 2
    mate = t + 1 - 2 * core
    heads, seqs, seg, hd = qt_ref.shape
    tokens, width = x_ref.shape
    half = tokens // 2
    local_experts = wg.shape[0]
    ch = width // n_tp
    pp = seg // n_tp

    weights = [
        pltpu.make_async_copy(src, dst, w_sem.at[i])
        for i, (src, dst) in enumerate(
            ((gate_hbm, wg), (up_hbm, wu), (down_hbm, wd), (mixer_hbm, wm))
        )
    ]
    for copy in weights:
        copy.start()

    def ep_peer(d):
        return partner_of(e, d, n_ep)

    barrier = pltpu.get_barrier_semaphore()
    for d in range(1, n_ep):
        pl.semaphore_signal(barrier, inc=1, device_id={"ep": ep_peer(d)}, device_id_type=MESH)
    for d in range(1, n_tp):
        pl.semaphore_signal(
            barrier, inc=1, device_id={"tp": (t + d) % n_tp}, device_id_type=MESH
        )
    pl.semaphore_wait(barrier, n_ep - 1 + n_tp - 1)

    mine = pl.ds(pl.multiple_of(core * half, half), half)

    def x_copy(d):
        return pltpu.make_async_remote_copy(
            src_ref=x_ref.at[mine],
            dst_ref=xr.at[d, mine],
            send_sem=x_ss.at[d],
            recv_sem=x_rs.at[d],
            device_id={"ep": ep_peer(d)},
            device_id_type=MESH,
        )

    def wt_copy(d):
        return pltpu.make_async_remote_copy(
            src_ref=wt_ref.at[ep_peer(d)],
            dst_ref=wr.at[d],
            send_sem=wt_ss.at[d],
            recv_sem=wt_rs.at[d],
            device_id={"ep": ep_peer(d)},
            device_id_type=MESH,
        )

    def f_copy(d):
        return pltpu.make_async_remote_copy(
            src_ref=xr.at[d, mine],
            dst_ref=xr.at[d, mine],
            send_sem=f_ss.at[d],
            recv_sem=f_rs.at[d],
            device_id={"tp": mate},
            device_id_type=MESH,
        )

    def kv_copy(d):
        return pltpu.make_async_remote_copy(
            src_ref=kv_ref,
            dst_ref=kvr.at[d],
            send_sem=kv_ss.at[d],
            recv_sem=kv_rs.at[d],
            device_id={"ep": (e + d) % n_ep},
            device_id_type=MESH,
        )

    def c_copy(d):
        return pltpu.make_async_remote_copy(
            src_ref=pb.at[d, 1 - core],
            dst_ref=cr.at[d],
            send_sem=c_ss.at[d],
            recv_sem=c_rs.at[d],
            device_id={"tp": mate},
            device_id_type=MESH,
        )

    def r_copy(d):
        return pltpu.make_async_remote_copy(
            src_ref=sb.at[d],
            dst_ref=rr.at[d],
            send_sem=r_ss.at[d],
            recv_sem=r_rs.at[d],
            device_id={"ep": ep_peer(d)},
            device_id_type=MESH,
        )

    def z_copy(d):
        dz = (zi + d) % zs
        return pltpu.make_async_remote_copy(
            src_ref=zb.at[dz],
            dst_ref=zr.at[d],
            send_sem=z_ss.at[d],
            recv_sem=z_rs.at[d],
            device_id={"tp": dz * 2 + core},
            device_id_type=MESH,
        )

    def a_copy(d):
        to = (t + d) % n_tp
        return pltpu.make_async_remote_copy(
            src_ref=at_send.at[to],
            dst_ref=at_recv.at[t],
            send_sem=a_ss.at[d],
            recv_sem=a_rs.at[d],
            device_id={"tp": to},
            device_id_type=MESH,
        )

    for d in range(1, n_ep):
        wt_copy(d).start()
        x_copy(d).start()
    for d in range(1, n_ep):

        @pl.when(e + d < n_ep)
        def _():
            kv_copy(d).start()

    def normalize(rows_ref):
        values = rows_ref[...].astype(f32)
        mean = jnp.mean(values * values, axis=-1, keepdims=True)
        xn[...] = (values * lax.rsqrt(mean + norm_eps) * gain_ref[...]).astype(bf16)

    def experts(d, route):
        columns = route.T
        hidden = []
        for j in range(local_experts):
            gate_pre = jnp.dot(xn[...], wg[j], preferred_element_type=f32)
            up_pre = jnp.dot(xn[...], wu[j], preferred_element_type=f32)
            hidden.append(activate(gate_pre, up_pre))
        for c in range(n_tp):
            total = None
            for j in range(local_experts):
                term = columns[:, j : j + 1] * jnp.dot(
                    hidden[j], wd[j, :, c * ch : (c + 1) * ch], preferred_element_type=f32
                )
                total = term if total is None else total + term
            pb[d, c % 2, c // 2] = total.astype(bf16)

    def finish(d):
        c_copy(d).wait_recv()
        sb[d] = (pb[d, core].astype(f32) + cr[d].astype(f32)).astype(bf16)

    normalize(x_ref)
    for copy in weights[:3]:
        copy.wait()
    experts(0, wt_ref[e])
    c_copy(0).start()

    def step(d, carry):
        x_copy(d).wait_recv()
        f_copy(d).start()
        finish(d - 1)

        @pl.when(d > 1)
        def _():
            r_copy(d - 1).start()

        f_copy(d).wait_recv()
        wt_copy(d).wait_recv()
        normalize(xr.at[d])
        experts(d, wr[d])
        c_copy(d).start()
        return carry

    lax.fori_loop(1, n_ep, step, 0)
    finish(n_ep - 1)
    r_copy(n_ep - 1).start()

    pairs = heads * seqs
    row_id = lax.broadcasted_iota(jnp.int32, (seg, seg), 0)
    col_id = lax.broadcasted_iota(jnp.int32, (seg, seg), 1)
    later_mask = (row_id > col_id).astype(f32).astype(bf16)
    scale = hd ** (-0.5)

    def block(kv, diagonal):
        outs = []
        for p in range(pairs):
            h, s = p // seqs, p % seqs
            scores = jnp.dot(qt_ref[h, s], kv[0, h, s], preferred_element_type=f32) * scale
            log_term = jnp.log(1.0 + jnp.exp(-jnp.abs(scores)))
            keep = -(jnp.maximum(scores, 0.0) + log_term)
            beta = jnp.minimum(scores, 0.0) - log_term
            if diagonal:
                keep = jnp.where(col_id < row_id, keep, 0.0)
            high = keep.astype(bf16)
            low = (keep - high.astype(f32)).astype(bf16)
            within = jnp.dot(high, later_mask, preferred_element_type=f32) + jnp.dot(
                low, later_mask, preferred_element_type=f32
            )
            weight = jnp.exp(beta + within)
            if diagonal:
                weight = jnp.where(col_id < row_id, weight, 0.0)
            out = lax.dot_general(
                weight.astype(bf16),
                kv[1, h, s],
                (((1,), (1,)), ((), ())),
                preferred_element_type=f32,
            )
            outs.append((out, jnp.sum(keep, axis=1, keepdims=True)))
        return outs

    first = block(kv_ref, True)
    state = []
    for out, total in first:
        state.extend((out, total))

    def further(d, state):
        pltpu.make_async_remote_copy(
            src_ref=kv_ref,
            dst_ref=kvr.at[d],
            send_sem=kv_ss.at[d],
            recv_sem=kv_rs.at[d],
            device_id={"ep": (e + d) % n_ep},
            device_id_type=MESH,
        ).wait_recv()
        fresh = []
        for p, (out, total) in enumerate(block(kvr.at[d], False)):
            so_far, later = state[2 * p], state[2 * p + 1]
            fresh.extend((so_far + jnp.exp(later) * out, later + total))
        return tuple(fresh)

    state = lax.fori_loop(1, e + 1, further, tuple(state))
    for p in range(pairs):
        h, s = p // seqs, p % seqs
        attended = state[2 * p]
        for c in range(n_tp):
            at_send[c, s * pp : (s + 1) * pp, h * hd : (h + 1) * hd] = attended[
                c * pp : (c + 1) * pp
            ].astype(bf16)
    for d in range(1, n_tp):
        a_copy(d).start()

    for d in range(1, n_ep):
        r_copy(d).wait_recv()
    for c in range(zs):
        total = sb[0, c].astype(f32)
        for d in range(1, n_ep):
            total = total + rr[d, c].astype(f32)
        zb[c] = total.astype(bf16)
    for d in range(1, zs):
        z_copy(d).start()

    weights[3].wait()
    at_recv[t] = at_send[t]
    for d in range(1, n_tp):
        pltpu.make_async_remote_copy(
            src_ref=at_send.at[t],
            dst_ref=at_recv.at[(t + n_tp - d) % n_tp],
            send_sem=a_ss.at[d],
            recv_sem=a_rs.at[d],
            device_id={"tp": (t + d) % n_tp},
            device_id_type=MESH,
        ).wait_recv()
    channels = heads * hd
    wide = jnp.concatenate([at_recv[c] for c in range(n_tp)], axis=1)
    mixed = jnp.dot(wide, wm[...], preferred_element_type=f32)
    for s in range(seqs):
        mix_out[s] = mixed[s * pp : (s + 1) * pp].astype(bf16)

    total = zb[zi].astype(f32)
    for d in range(1, zs):
        z_copy(d).wait_recv()
        total = total + zr[d].astype(f32)
    routed_out[...] = total.T.astype(bf16)

    for d in range(1, n_ep):
        x_copy(d).wait_send()
        wt_copy(d).wait_send()
        f_copy(d).wait_send()
        r_copy(d).wait_send()

        @pl.when(e + d < n_ep)
        def _():
            kv_copy(d).wait_send()

    for d in range(n_ep):
        c_copy(d).wait_send()
    for d in range(1, zs):
        z_copy(d).wait_send()
    for d in range(1, n_tp):
        a_copy(d).wait_send()


def body(
    queries,
    key_vectors,
    value_vectors,
    mixer_weight,
    expert_rows,
    norm_gain,
    route_ids,
    route_logits,
    gate_weight,
    up_weight,
    down_weight,
):
    n_ep, n_tp = lax.axis_size("ep"), lax.axis_size("tp")
    heads, hd, seqs, seg = queries.shape
    tokens, width = expert_rows.shape
    local_experts, _, ff = gate_weight.shape
    zs, ch, pp = n_tp // 2, width // n_tp, seg // n_tp

    qt = queries.transpose(0, 2, 3, 1)
    kv = jnp.stack([key_vectors, value_vectors]).transpose(0, 1, 3, 2, 4)
    route_weight = jax.nn.softmax(route_logits, axis=-1)
    slots = 8 * -(-local_experts // 8)
    expert = (
        jnp.arange(n_ep, dtype=jnp.int32)[:, None] * local_experts
        + jnp.arange(slots, dtype=jnp.int32)[None, :]
    )
    inside = jnp.arange(slots, dtype=jnp.int32)[None, :, None] < local_experts
    table = 0.0
    for k in range(route_ids.shape[1]):
        hit = jnp.logical_and(route_ids[:, k][None, None, :] == expert[:, :, None], inside)
        table = table + jnp.where(hit, route_weight[:, k][None, None, :], 0.0)

    vmem = pl.BlockSpec(memory_space=pltpu.VMEM)
    anywhere = pl.BlockSpec(memory_space=pl.ANY)
    dma = pltpu.SemaphoreType.DMA
    return pl.pallas_call(
        functools.partial(kernel, n_ep, n_tp),
        out_shape=(
            jax.ShapeDtypeStruct((seqs, pp, width), bf16),
            jax.ShapeDtypeStruct((ch, tokens), bf16),
        ),
        in_specs=[vmem] * 5 + [anywhere] * 4,
        out_specs=(vmem, vmem),
        scratch_shapes=[
            pltpu.VMEM(gate_weight.shape, bf16),
            pltpu.VMEM(up_weight.shape, bf16),
            pltpu.VMEM(down_weight.shape, bf16),
            pltpu.VMEM(mixer_weight.shape, bf16),
            pltpu.VMEM((n_ep, tokens, width), bf16),
            pltpu.VMEM((n_ep, slots, tokens), f32),
            pltpu.VMEM((tokens, width), bf16),
            pltpu.VMEM((n_ep,) + kv.shape, bf16),
            pltpu.VMEM((n_ep, 2, zs, tokens, ch), bf16),
            pltpu.VMEM((n_ep, zs, tokens, ch), bf16),
            pltpu.VMEM((n_ep, zs, tokens, ch), bf16),
            pltpu.VMEM((n_ep, zs, tokens, ch), bf16),
            pltpu.VMEM((zs, tokens, ch), bf16),
            pltpu.VMEM((zs, tokens, ch), bf16),
            pltpu.VMEM((n_tp, seqs * pp, heads * hd), bf16),
            pltpu.VMEM((n_tp, seqs * pp, heads * hd), bf16),
            dma((4,)),
        ]
        + [dma((n_ep,))] * 12
        + [dma((zs,))] * 2
        + [dma((n_tp,))] * 2,
        compiler_params=pltpu.CompilerParams(
            collective_id=0, has_side_effects=True, vmem_limit_bytes=60 * 1024 * 1024
        ),
    )(
        qt,
        kv,
        expert_rows,
        norm_gain[None, :],
        table,
        gate_weight,
        up_weight,
        down_weight,
        mixer_weight,
    )


def solution(mesh):
    in_specs = (
        P("tp", None, None, "ep"),
        P("tp", None, None, "ep"),
        P("tp", None, None, "ep"),
        P(),
        P("ep", None),
        P(),
        P("ep", None),
        P("ep", None),
        P("ep", None, "tp"),
        P("ep", None, "tp"),
        P("ep", "tp", None),
    )
    out_specs = (P(None, ("ep", "tp"), None), P("tp", "ep"))
    return jax.shard_map(body, mesh=mesh, in_specs=in_specs, out_specs=out_specs, check_vma=False)
```

time: 131 us -> 58.6 us (0.45)
  blocking collectives: 48.1 us -> 0 us
  Pallas kernels: 0 us -> 47.8 us
  starting transfers between devices: 23.5 us -> 0 us
  between operations: 14.3 us -> 0.66 us
  matrix products: 13.1 us -> 0 us
  local copies, waits for them, and re-layouts: 14.2 us -> 6.3 us
  waiting for transfers between devices: 7.31 us -> 0 us
  other arithmetic: 9.63 us -> 3.5 us
    pallas_call x0 -> x1, Pallas kernels: none -> 47.8 us  [body(): pl.pallas_call(functools.partial(kernel, n_ep, n_tp), out_shape=(jax.Shap...]
    all_to_all x1 -> x0, blocking collectives: 30.6 us -> none  [expert_block(): lax.all_to_all(send_rows, 'ep', split_axis=0, concat_axis=0, tiled=True)]
    all_to_all x2 -> x0, starting transfers between devices: 23.4 us -> none  [the longest x1 18.6 us: expert_block(): lax.all_to_all(summed.astype(jnp.bfloat16), 'ep', split_axis=1, concat_ax...]
    all_gather x2 -> x0, blocking collectives: 17.5 us -> none  [the longest x1 8.89 us: attend(): value_piece = lax.all_gather(value_vectors, 'ep', axis=3, tiled=True)]
    dot_general x5 -> x0, matrix products: 13.1 us -> none  [the longest x1 7.28 us: expert_block(): jnp.einsum('sjcf,jfd->dsjc', hidden, down_part, preferred_element_type=jn...]
    all_to_all x2 -> x0, waiting for transfers between devices: 7.04 us -> none  [the longest x1 5.35 us: mix_heads(): lax.all_to_all(flat_heads, 'tp', split_axis=2, concat_axis=0, tiled=True)]
    another operation x4 -> x0, other arithmetic: 5.06 us -> none  [the longest x1 4.43 us: block_terms(): within = lax.cumsum(log_keep, axis=3, reverse=True) - log_keep]
    convert_element_type x3 -> x0, local copies, waits for them, and re-layouts: 3.96 us -> none  [the longest x1 3.19 us: expert_block(): summed = lax.psum_scatter(term_rows.reshape(model_width // lax.axis_size(...]
  transfers between devices with their start and end apart: 3 -> 0, of which waited for: 3 -> 0; matrix products, arithmetic and copies ran while one was open for 8% -> 0% of each run, Pallas kernels for 0% -> 0%
where the time goes in v1:
time: 58.6 us; the launch traced here: 58.2 us
  Pallas kernels  47.8 us (82%)
  local copies, waits for them, and re-layouts  6.3 us (11%)
  other arithmetic  3.5 us (6%)
  between operations  0.66 us (1%)
    pallas_call x1, Pallas kernels, body(): pl.pallas_call(functools.partial(kernel, n_ep, n_tp), out_shape=(jax.Shap...  47.8 us
    unnamed x3, local copies, waits for them, and re-layouts  4.65 us

profile of v1, /device:TPU:0, one launch (start us, length us, event | category | flops | bytes accessed | tf_op | source)
XLA Modules:
  0.0 58.2 jit_solution(16630270651093153488)
XLA Ops:
  0.6 0.7 %reduce_max.9 = f32[128]{0:T(128)S(1)} reduce(f32[128,2]{0,1:T(2,128)} %param.18, f32[]{:T(128)} %constant.4.clone.1), dimensions={1}, to_apply=%region_0.0 | reduce | flops 128 | bytes 1540 | tf_op jit(solution)/shard_map/reduce_max | solution.py:397
  1.3 0.7 %fusion.1 = f32[128]{0:T(128)S(1)} fusion(f32[128,2]{0,1:T(2,128)} %param.18, f32[128]{0:T(128)S(1)} %reduce_max.9), kind=kLoop, calls=%fused_computation.7 | loop fusion | flops 384 | bytes 2048 | tf_op jit(solution)/shard_map/reduce_sum | solution.py:397
  2.0 0.7 %fusion = f32[128,2]{0,1:T(2,128)S(1)} fusion(f32[128,2]{0,1:T(2,128)} %param.18, f32[128]{0:T(128)S(1)} %fusion.1, f32[128]{0:T(128)S(1)} %reduce_max.9), kind=kLoop, calls=%fused_computation.6 | loop fusion | flops 512 | bytes 3072 | tf_op jit(solution)/shard_map/div | solution.py:397
  2.7 0.8 %slice_bitcast_fusion.3 = (s32[128]{0:T(128)S(1)}, s32[128]{0:T(128)S(1)}) fusion(s32[128,2]{0,1:T(2,128)} %param.17), kind=kLoop, calls=%fused_computation.13 | loop fusion | bytes 2048 | tf_op jit(solution)/shard_map/eq | solution.py:406
  3.5 0.1 iota_add_fusion
  3.6 0.7 %select_add_fusion.wt_ref = f32[4,8,128]{2,1,0:T(8,128)} fusion(f32[128]{0:T(128)S(1)} %get-tuple-element.5, s32[128]{0:T(128)S(1)} %get-tuple-element.3, f32[128]{0:T(128)S(1)} %get-tuple-element.4, s32[4,8]{1,0:T(4,128)S(1)} %iota_add_fusion, s32[128]{0:T(128)S(1)} %get-tuple-element.2, pred[8]{0:T(512)(128)(4,1)S(1)} %iota_compare_fusion), kind=kLoop, calls=%fused_computation.3 | loop fusion | flops 28672 | bytes 18568 | tf_op jit(solution)/shard_map/add | solution.py:407
  4.3 1.6 %copy.13 = bf16[2,64,2,128]{1,3,2,0:T(8,128)(2,1)} copy(bf16[2,64,2,128]{3,2,1,0:T(2,128)(2,1)} %param.11) | data formatting | bytes 131072 | tf_op args[0]
  5.9 0.9 %copy_bitcast_fusion = (bf16[1,2,64,2,128]{4,2,3,1,0:T(8,128)(2,1)S(1)}, bf16[1,2,64,2,128]{4,2,3,1,0:T(8,128)(2,1)S(1)}) fusion(bf16[2,64,2,128]{3,2,1,0:T(2,128)(2,1)} %param.13, bf16[2,64,2,128]{3,2,1,0:T(2,128)(2,1)} %param.12), kind=kLoop, calls=%fused_computation.1 | loop fusion | bytes 262144 | tf_op jit(solution)/shard_map/stack | solution.py:396
  6.8 0.7 %maximum_bitcast_fusion.kv_ref = bf16[2,2,2,64,128]{4,3,2,1,0:T(8,128)(2,1)} fusion(bf16[1,2,64,2,128]{4,2,3,1,0:T(8,128)(2,1)S(1)} %get-tuple-element.6, bf16[1,2,64,2,128]{4,2,3,1,0:T(8,128)(2,1)S(1)} %get-tuple-element.7), kind=kLoop, calls=%fused_computation | loop fusion | flops 65536 | bytes 262144 | tf_op jit(solution)/shard_map/transpose | solution.py:396
  7.4 47.8 %shard_map.122 = (bf16[2,16,2048]{2,1,0:T(8,128)(2,1)}, bf16[256,128]{1,0:T(8,128)(2,1)}) custom-call(bf16[2,2,128,64]{3,2,1,0:T(8,128)(2,1)} %bitcast.16, bf16[2,2,2,64,128]{4,3,2,1,0:T(8,128)(2,1)} %maximum_bitcast_fusion.kv_ref, bf16[128,2048]{1,0:T(8,128)(2,1)} %x_ref.1, f32[1,2048]{1,0:T(1,128)} %bitcast.17, f32[4,8,128]{2,1,0:T(8,128)} %select_add_fusion.wt_ref, ...), custom_call_target="tpu_custom_call" | custom-call | tf_op jit(solution)/shard_map/pallas_call | solution.py:412
  55.2 1.6 %copy.20 = bf16[2,16,2048]{2,1,0:T(8,128)(2,1)} copy(bf16[2,16,2048]{2,1,0:T(8,128)(2,1)} %get-tuple-element.10) | data formatting | bytes 262144
  56.8 1.5 %copy.21 = bf16[256,128]{1,0:T(8,128)(2,1)} copy(bf16[256,128]{1,0:T(8,128)(2,1)} %get-tuple-element.11) | data formatting | bytes 131072
  (3 shorter events, 0.0 us)

commit v2 on v1

--- a/solution.py
+++ b/solution.py
@@ -35,11 +35,13 @@
 def kernel(
     n_ep,
     n_tp,
-    qt_ref,
-    kv_ref,
+    q_ref,
+    k_ref,
+    v_ref,
     x_ref,
     gain_ref,
-    wt_ref,
+    ids_ref,
+    logits_ref,
     gate_hbm,
     up_hbm,
     down_hbm,
@@ -62,11 +64,18 @@
     zr,
     at_send,
     at_recv,
+    qt_ref,
+    kv_ref,
+    wt_ref,
+    acc,
+    tot,
     w_sem,
     x_ss,
     x_rs,
     wt_ss,
     wt_rs,
+    g_ss,
+    g_rs,
     f_ss,
     f_rs,
     kv_ss,
@@ -89,6 +98,10 @@
     heads, seqs, seg, hd = qt_ref.shape
     tokens, width = x_ref.shape
     half = tokens // 2
+    quarter = tokens // 4
+    zp = zi % 2
+    zmate = t + 2 - 4 * zp
+    slots = wt_ref.shape[1]
     local_experts = wg.shape[0]
     ch = width // n_tp
     pp = seg // n_tp
@@ -112,14 +125,45 @@
         pl.semaphore_signal(
             barrier, inc=1, device_id={"tp": (t + d) % n_tp}, device_id_type=MESH
         )
+
+    rows = hd * seqs
+    for s in range(seqs):
+        pick = (
+            lax.broadcasted_iota(jnp.int32, (hd, rows), 1)
+            == lax.broadcasted_iota(jnp.int32, (hd, rows), 0) * seqs + s
+        ).astype(f32).astype(bf16)
+        for h in range(heads):
+            kv_ref[0, h, s] = jnp.dot(pick, k_ref[h], preferred_element_type=f32).astype(bf16)
+            kv_ref[1, h, s] = jnp.dot(pick, v_ref[h], preferred_element_type=f32).astype(bf16)
+            query = jnp.dot(pick, q_ref[h], preferred_element_type=f32)
+            qt_ref[h, s] = query.T.astype(bf16)
+
+    top = ids_ref.shape[0]
+    logits = [logits_ref[k : k + 1] for k in range(top)]
+    peak = functools.reduce(jnp.maximum, logits)
+    powers = [jnp.exp(value - peak) for value in logits]
+    share = 1.0 / functools.reduce(jnp.add, powers)
+    slot = lax.broadcasted_iota(jnp.int32, (slots, tokens), 0)
+    for group in range(n_ep):
+        expert = jnp.where(slot < local_experts, group * local_experts + slot, -1)
+        table = jnp.zeros((slots, tokens), f32)
+        for k in range(top):
+            table = table + jnp.where(ids_ref[k : k + 1] == expert, powers[k] * share, 0.0)
+        wt_ref[group] = table
     pl.semaphore_wait(barrier, n_ep - 1 + n_tp - 1)
 
     mine = pl.ds(pl.multiple_of(core * half, half), half)
 
-    def x_copy(d):
-        return pltpu.make_async_remote_copy(
-            src_ref=x_ref.at[mine],
-            dst_ref=xr.at[d, mine],
+    piece = pl.ds(pl.multiple_of(core * half + zp * quarter, quarter), quarter)
+
+    def far(d):
+        return sum((d // 2**i) % 2 for i in range(n_ep.bit_length())) > 1
+
+    def x_copy(d, is_far):
+        sent = piece if is_far else mine
+        return pltpu.make_async_remote_copy(
+            src_ref=x_ref.at[sent],
+            dst_ref=xr.at[d, sent],
             send_sem=x_ss.at[d],
             recv_sem=x_rs.at[d],
             device_id={"ep": ep_peer(d)},
@@ -136,6 +180,16 @@
             device_id_type=MESH,
         )
 
+    def g_copy(d):
+        return pltpu.make_async_remote_copy(
+            src_ref=xr.at[d, piece],
+            dst_ref=xr.at[d, piece],
+            send_sem=g_ss.at[d],
+            recv_sem=g_rs.at[d],
+            device_id={"tp": zmate},
+            device_id_type=MESH,
+        )
+
     def f_copy(d):
         return pltpu.make_async_remote_copy(
             src_ref=xr.at[d, mine],
@@ -166,12 +220,13 @@
             device_id_type=MESH,
         )
 
-    def r_copy(d):
-        return pltpu.make_async_remote_copy(
-            src_ref=sb.at[d],
-            dst_ref=rr.at[d],
-            send_sem=r_ss.at[d],
-            recv_sem=r_rs.at[d],
+    def r_copy(d, k):
+        c = (zi + k) % zs
+        return pltpu.make_async_remote_copy(
+            src_ref=sb.at[d, c],
+            dst_ref=rr.at[d, c],
+            send_sem=r_ss.at[d, k - 1],
+            recv_sem=r_rs.at[d, k - 1],
             device_id={"ep": ep_peer(d)},
             device_id_type=MESH,
         )
@@ -200,7 +255,10 @@
 
     for d in range(1, n_ep):
         wt_copy(d).start()
-        x_copy(d).start()
+    distances = [d for d in range(1, n_ep) if far(d)]
+    near = [d for d in range(1, n_ep) if not far(d)]
+    for d in distances + near:
+        x_copy(d, far(d)).start()
     for d in range(1, n_ep):
 
         @pl.when(e + d < n_ep)
@@ -228,35 +286,13 @@
                 total = term if total is None else total + term
             pb[d, c % 2, c // 2] = total.astype(bf16)
 
-    def finish(d):
+    def finish(d, send):
         c_copy(d).wait_recv()
-        sb[d] = (pb[d, core].astype(f32) + cr[d].astype(f32)).astype(bf16)
-
-    normalize(x_ref)
-    for copy in weights[:3]:
-        copy.wait()
-    experts(0, wt_ref[e])
-    c_copy(0).start()
-
-    def step(d, carry):
-        x_copy(d).wait_recv()
-        f_copy(d).start()
-        finish(d - 1)
-
-        @pl.when(d > 1)
-        def _():
-            r_copy(d - 1).start()
-
-        f_copy(d).wait_recv()
-        wt_copy(d).wait_recv()
-        normalize(xr.at[d])
-        experts(d, wr[d])
-        c_copy(d).start()
-        return carry
-
-    lax.fori_loop(1, n_ep, step, 0)
-    finish(n_ep - 1)
-    r_copy(n_ep - 1).start()
+        for k in range(1, zs + 1):
+            c = (zi + k) % zs
+            sb[d, c] = (pb[d, core, c].astype(f32) + cr[d, c].astype(f32)).astype(bf16)
+            if send:
+                r_copy(d, k).start()
 
     pairs = heads * seqs
     row_id = lax.broadcasted_iota(jnp.int32, (seg, seg), 0)
@@ -291,30 +327,60 @@
             outs.append((out, jnp.sum(keep, axis=1, keepdims=True)))
         return outs
 
-    first = block(kv_ref, True)
-    state = []
-    for out, total in first:
-        state.extend((out, total))
-
-    def further(d, state):
-        pltpu.make_async_remote_copy(
-            src_ref=kv_ref,
-            dst_ref=kvr.at[d],
-            send_sem=kv_ss.at[d],
-            recv_sem=kv_rs.at[d],
-            device_id={"ep": (e + d) % n_ep},
-            device_id_type=MESH,
-        ).wait_recv()
-        fresh = []
+    for p, (out, total) in enumerate(block(kv_ref, True)):
+        acc[p] = out
+        tot[p] = total
+
+    normalize(x_ref)
+    for d in distances:
+        x_copy(d, True).wait_recv()
+        g_copy(d).start()
+    for copy in weights[:3]:
+        copy.wait()
+    experts(0, wt_ref[e])
+    c_copy(0).start()
+
+    def step(d, carry):
+        @pl.when(far(d))
+        def _():
+            g_copy(d).wait_recv()
+
+        @pl.when(jnp.logical_not(far(d)))
+        def _():
+            x_copy(d, False).wait_recv()
+
+        f_copy(d).start()
+
+        @pl.when(d == 1)
+        def _():
+            finish(0, False)
+
+        @pl.when(d > 1)
+        def _():
+            finish(d - 1, True)
+
+        f_copy(d).wait_recv()
+        wt_copy(d).wait_recv()
+        normalize(xr.at[d])
+        experts(d, wr[d])
+        c_copy(d).start()
+        return carry
+
+    lax.fori_loop(1, n_ep, step, 0)
+    finish(n_ep - 1, True)
+
+    def further(d, carry):
+        kv_copy(d).wait_recv()
         for p, (out, total) in enumerate(block(kvr.at[d], False)):
-            so_far, later = state[2 * p], state[2 * p + 1]
-            fresh.extend((so_far + jnp.exp(later) * out, later + total))
-        return tuple(fresh)
-
-    state = lax.fori_loop(1, e + 1, further, tuple(state))
+            later = tot[p]
+            acc[p] = acc[p] + jnp.exp(later) * out
+            tot[p] = later + total
+        return carry
+
+    lax.fori_loop(1, e + 1, further, 0)
     for p in range(pairs):
         h, s = p // seqs, p % seqs
-        attended = state[2 * p]
+        attended = acc[p]
         for c in range(n_tp):
             at_send[c, s * pp : (s + 1) * pp, h * hd : (h + 1) * hd] = attended[
                 c * pp : (c + 1) * pp
@@ -322,15 +388,16 @@
     for d in range(1, n_tp):
         a_copy(d).start()
 
-    for d in range(1, n_ep):
-        r_copy(d).wait_recv()
-    for c in range(zs):
-        total = sb[0, c].astype(f32)
+    own = None
+    for k in range(1, zs + 1):
+        c = (zi + k) % zs
+        own = sb[0, c].astype(f32)
         for d in range(1, n_ep):
-            total = total + rr[d, c].astype(f32)
-        zb[c] = total.astype(bf16)
-    for d in range(1, zs):
-        z_copy(d).start()
+            r_copy(d, k).wait_recv()
+            own = own + rr[d, c].astype(f32)
+        if k < zs:
+            zb[c] = own.astype(bf16)
+            z_copy(k).start()
 
     weights[3].wait()
     at_recv[t] = at_send[t]
@@ -349,17 +416,20 @@
     for s in range(seqs):
         mix_out[s] = mixed[s * pp : (s + 1) * pp].astype(bf16)
 
-    total = zb[zi].astype(f32)
+    total = own
     for d in range(1, zs):
         z_copy(d).wait_recv()
         total = total + zr[d].astype(f32)
     routed_out[...] = total.T.astype(bf16)
 
     for d in range(1, n_ep):
-        x_copy(d).wait_send()
+        x_copy(d, far(d)).wait_send()
+        if far(d):
+            g_copy(d).wait_send()
         wt_copy(d).wait_send()
         f_copy(d).wait_send()
-        r_copy(d).wait_send()
+        for k in range(1, zs + 1):
+            r_copy(d, k).wait_send()
 
         @pl.when(e + d < n_ep)
         def _():
@@ -392,30 +462,26 @@
     local_experts, _, ff = gate_weight.shape
     zs, ch, pp = n_tp // 2, width // n_tp, seg // n_tp
 
-    qt = queries.transpose(0, 2, 3, 1)
-    kv = jnp.stack([key_vectors, value_vectors]).transpose(0, 1, 3, 2, 4)
-    route_weight = jax.nn.softmax(route_logits, axis=-1)
+    top = route_ids.shape[1]
     slots = 8 * -(-local_experts // 8)
-    expert = (
-        jnp.arange(n_ep, dtype=jnp.int32)[:, None] * local_experts
-        + jnp.arange(slots, dtype=jnp.int32)[None, :]
-    )
-    inside = jnp.arange(slots, dtype=jnp.int32)[None, :, None] < local_experts
-    table = 0.0
-    for k in range(route_ids.shape[1]):
-        hit = jnp.logical_and(route_ids[:, k][None, None, :] == expert[:, :, None], inside)
-        table = table + jnp.where(hit, route_weight[:, k][None, None, :], 0.0)
+    pairs = heads * seqs
+    kv_shape = (2, heads, seqs, hd, seg)
+
+    def merged(rows):
+        return rows.reshape(heads, hd * seqs, seg)
 
     vmem = pl.BlockSpec(memory_space=pltpu.VMEM)
-    anywhere = pl.BlockSpec(memory_space=pl.ANY)
+    anywhere = pl.BlockSpec(memory_space=pltpu.HBM)
     dma = pltpu.SemaphoreType.DMA
+    outs = 2 * seqs * pp * width + 2 * ch * tokens
+    limit = (60 * 1024 * 1024) - outs - (64 << 10)
     return pl.pallas_call(
         functools.partial(kernel, n_ep, n_tp),
         out_shape=(
             jax.ShapeDtypeStruct((seqs, pp, width), bf16),
             jax.ShapeDtypeStruct((ch, tokens), bf16),
         ),
-        in_specs=[vmem] * 5 + [anywhere] * 4,
+        in_specs=[vmem] * 7 + [anywhere] * 4,
         out_specs=(vmem, vmem),
         scratch_shapes=[
             pltpu.VMEM(gate_weight.shape, bf16),
@@ -425,7 +491,7 @@
             pltpu.VMEM((n_ep, tokens, width), bf16),
             pltpu.VMEM((n_ep, slots, tokens), f32),
             pltpu.VMEM((tokens, width), bf16),
-            pltpu.VMEM((n_ep,) + kv.shape, bf16),
+            pltpu.VMEM((n_ep,) + kv_shape, bf16),
             pltpu.VMEM((n_ep, 2, zs, tokens, ch), bf16),
             pltpu.VMEM((n_ep, zs, tokens, ch), bf16),
             pltpu.VMEM((n_ep, zs, tokens, ch), bf16),
@@ -434,20 +500,28 @@
             pltpu.VMEM((zs, tokens, ch), bf16),
             pltpu.VMEM((n_tp, seqs * pp, heads * hd), bf16),
             pltpu.VMEM((n_tp, seqs * pp, heads * hd), bf16),
+            pltpu.VMEM((heads, seqs, seg, hd), bf16),
+            pltpu.VMEM(kv_shape, bf16),
+            pltpu.VMEM((n_ep, slots, tokens), f32),
+            pltpu.VMEM((pairs, seg, hd), f32),
+            pltpu.VMEM((pairs, seg, 1), f32),
             dma((4,)),
         ]
         + [dma((n_ep,))] * 12
+        + [dma((n_ep, zs))] * 2
         + [dma((zs,))] * 2
         + [dma((n_tp,))] * 2,
         compiler_params=pltpu.CompilerParams(
-            collective_id=0, has_side_effects=True, vmem_limit_bytes=60 * 1024 * 1024
+            collective_id=0, has_side_effects=True, vmem_limit_bytes=limit
         ),
     )(
-        qt,
-        kv,
+        merged(queries),
+        merged(key_vectors),
+        merged(value_vectors),
         expert_rows,
         norm_gain[None, :],
-        table,
+        route_ids.T,
+        route_logits.T,
         gate_weight,
         up_weight,
         down_weight,

time: 58.6 us -> 46.7 us (0.80)
  Pallas kernels: 47.8 us -> 42.8 us
  other arithmetic: 3.5 us -> 0 us
  local copies, waits for them, and re-layouts: 6.3 us -> 3.04 us
    pallas_call x1, Pallas kernels: 47.8 us -> 42.8 us  [body(): pl.pallas_call(functools.partial(kernel, n_ep, n_tp), out_shape=(jax.Shap...]
    unnamed x3 -> x2, local copies, waits for them, and re-layouts: 4.65 us -> 3.04 us
    another operation x1 -> x0, local copies, waits for them, and re-layouts: 0.89 us -> none  [body(): kv = jnp.stack([key_vectors, value_vectors]).transpose(0, 1, 3, 2, 4)]
    eq x1 -> x0, local copies, waits for them, and re-layouts: 0.76 us -> none  [body(): route_ids[:, k][None, None, :] == expert[:, :, None]]
    add x2 -> x0, other arithmetic: 0.76 us -> none  [the longest x1 0.69 us: body(): table = table + jnp.where(hit, route_weight[:, k][None, None, :], 0.0)]
    reduce_max x1 -> x0, other arithmetic: 0.7 us -> none  [body(): route_weight = jax.nn.softmax(route_logits, axis=-1)]
    reduce_sum x1 -> x0, other arithmetic: 0.7 us -> none  [body(): route_weight = jax.nn.softmax(route_logits, axis=-1)]
    div x1 -> x0, other arithmetic: 0.69 us -> none  [body(): route_weight = jax.nn.softmax(route_logits, axis=-1)]
where the time goes in v2:
time: 46.7 us; the launch traced here: 46.5 us
  Pallas kernels  42.8 us (92%)
  local copies, waits for them, and re-layouts  3.04 us (7%)
  between operations  0.64 us (1%)
    pallas_call x1, Pallas kernels, body(): pl.pallas_call(functools.partial(kernel, n_ep, n_tp), out_shape=(jax.Shap...  42.8 us
    unnamed x2, local copies, waits for them, and re-layouts  3.04 us

profile of v2, /device:TPU:0, one launch (start us, length us, event | category | flops | bytes accessed | tf_op | source)
XLA Modules:
  0.0 46.5 jit_solution(4987377095686610103)
XLA Ops:
  0.6 42.8 %shard_map.122 = (bf16[2,16,2048]{2,1,0:T(8,128)(2,1)}, bf16[256,128]{1,0:T(8,128)(2,1)}) custom-call(bf16[2,128,128]{2,1,0:T(8,128)(2,1)} %bitcast.6, bf16[2,128,128]{2,1,0:T(8,128)(2,1)} %bitcast.7, bf16[2,128,128]{2,1,0:T(8,128)(2,1)} %bitcast.8, bf16[128,2048]{1,0:T(8,128)(2,1)} %x_ref.1, f32[1,2048]{1,0:T(1,128)} %bitcast.9, s32[2,128]{1,0:T(2,128)} %bitcast.10, ...), custom_call_target="tpu_custom_call" | custom-call | tf_op jit(solution)/shard_map/pallas_call | solution.py:478
  43.5 1.6 %copy.15 = bf16[2,16,2048]{2,1,0:T(8,128)(2,1)} copy(bf16[2,16,2048]{2,1,0:T(8,128)(2,1)} %get-tuple-element.4) | data formatting | bytes 262144
  45.0 1.5 %copy.16 = bf16[256,128]{1,0:T(8,128)(2,1)} copy(bf16[256,128]{1,0:T(8,128)(2,1)} %get-tuple-element.5) | data formatting | bytes 131072
